TPU v7x, 32 devices: a whole 2x2x4 slice. The times are simulated.
32 devices in a mesh: rep: 2 (over y), fs: 4 (over z), tp: 4 (over x, core).
Axes of the slice: x: 2, y: 2, z: 4, core: 2. Of those that a mesh axis runs over, the one named last changes fastest.
Arguments:
- activations: bfloat16 [3072, 2048], P(('rep', 'fs'), 'tp'), may hold values from -16 to 16
- norm_gain: float32 [2048], replicated, may hold values from 0.1 to 1.9
- query_weight: bfloat16 [2048, 512], P('fs', 'tp'), may hold values from -0.125 to 0.125
- key_weight: bfloat16 [2048, 512], P('fs', 'tp'), may hold values from -0.125 to 0.125
- value_weight: bfloat16 [2048, 512], P('fs', 'tp'), may hold values from -0.125 to 0.125
- gate_weight: bfloat16 [2048, 512], P('fs', 'tp'), may hold values from -0.125 to 0.125
- out_weight: bfloat16 [512, 2048], P('tp', 'fs'), may hold values from -0.25 to 0.25
- mlp_gain: float32 [2048], replicated, may hold values from 0.1 to 1.9
- up_weight: bfloat16 [2048, 8192], P('fs', 'tp'), may hold values from -0.125 to 0.125
- down_weight: bfloat16 [8192, 2048], P('tp', 'fs'), may hold values from -0.0625 to 0.0625
Outputs:
- layer_out: bfloat16 [3072, 2048], P(('rep', 'fs'), 'tp')
All inputs are finite; a program needn't handle non-finite values.
Results may differ from a plain program's by a relative error of at most 0.012.
Values may be sent and summed in bfloat16 or wider, within the bound.
A program may use at most 64 MiB of HBM per device.

v0:
```python
import jax
import jax.numpy as jnp
from jax import lax
from jax.sharding import PartitionSpec as P

HEADS = 8
HEAD_DIM = 64
BLOCK = 64
SEQ_LEN = 128
EPSILON = 1e-06


def rms_norm(rows, gain):
    floats = rows.astype(jnp.float32)
    scaled = floats * lax.rsqrt(jnp.mean(floats * floats, axis=-1, keepdims=True) + EPSILON)
    return (scaled * gain).astype(jnp.bfloat16)


def rotate(raw, cosine, sine, seqs, heads):
    half = HEAD_DIM // 2
    shaped = raw.reshape(seqs, SEQ_LEN, heads, HEAD_DIM)
    first, second = (shaped[..., :half], shaped[..., half:])
    return jnp.concatenate(
        [first * cosine - second * sine, second * cosine + first * sine], axis=-1
    )


def retain(query_raw, key_raw, value_rows, gate_rows, first_head):
    tokens = query_raw.shape[0]
    heads = query_raw.shape[1] // HEAD_DIM
    seqs = tokens // SEQ_LEN
    blocks = SEQ_LEN // BLOCK
    half = HEAD_DIM // 2
    position = jnp.arange(SEQ_LEN, dtype=jnp.float32)
    freqs = 10000.0 ** (-jnp.arange(half, dtype=jnp.float32) / half)
    angle = position[:, None] * freqs[None, :]
    cosine = jnp.cos(angle)[:, None, :]
    sine = jnp.sin(angle)[:, None, :]
    shape_five = (seqs, blocks, BLOCK, heads, HEAD_DIM)
    queries = rotate(query_raw, cosine, sine, seqs, heads).astype(jnp.bfloat16).reshape(shape_five)
    key_block = (
        (rotate(key_raw, cosine, sine, seqs, heads) * HEAD_DIM ** (-0.5))
        .astype(jnp.bfloat16)
        .reshape(shape_five)
    )
    value_block = value_rows.reshape(shape_five)
    head_index = first_head + jnp.arange(heads, dtype=jnp.float32)
    exponent = 5.0 + 4.0 * head_index / (HEADS - 1)
    log_gamma = jnp.log(1.0 - jnp.power(2.0, -exponent))
    offsets = jnp.arange(BLOCK, dtype=jnp.float32)
    distance = offsets[:, None] - offsets[None, :]
    decay_mask = jnp.where(
        distance[None] >= 0,
        jnp.exp(jnp.maximum(distance, 0.0)[None] * log_gamma[:, None, None]),
        0.0,
    )
    scores = jnp.einsum(
        "snbhd,snchd->snhbc", queries, key_block, preferred_element_type=jnp.float32
    )
    weights = (scores * decay_mask[None, None]).astype(jnp.bfloat16)
    inner = jnp.einsum(
        "snhbc,snchd->snbhd", weights, value_block, preferred_element_type=jnp.float32
    )
    query_decay = (
        queries.astype(jnp.float32)
        * jnp.exp((offsets + 1.0)[:, None] * log_gamma[None, :])[:, :, None]
    )
    key_decay = (
        key_block.astype(jnp.float32)
        * jnp.exp((BLOCK - 1.0 - offsets)[:, None] * log_gamma[None, :])[:, :, None]
    )
    block_decay = jnp.exp(BLOCK * log_gamma)[None, :, None, None]

    def advance(state, inputs):
        query_now, key_now, value_now = inputs
        carried = jnp.einsum("sbhd,shde->sbhe", query_now, state, precision=lax.Precision.HIGHEST)
        state = state * block_decay + jnp.einsum(
            "sbhd,sbhe->shde", key_now, value_now, precision=lax.Precision.HIGHEST
        )
        return (state, carried)

    initial = jnp.zeros((seqs, heads, HEAD_DIM, HEAD_DIM), jnp.float32)
    _, cross = lax.scan(
        advance,
        initial,
        (
            jnp.moveaxis(query_decay, 1, 0),
            jnp.moveaxis(key_decay, 1, 0),
            jnp.moveaxis(value_block.astype(jnp.float32), 1, 0),
        ),
    )
    mixed = (inner + jnp.moveaxis(cross, 0, 1)).reshape(tokens, heads, HEAD_DIM)
    centred = mixed - jnp.mean(mixed, axis=-1, keepdims=True)
    normed = centred * lax.rsqrt(jnp.mean(centred * centred, axis=-1, keepdims=True) + EPSILON)
    gated = normed * jax.nn.silu(gate_rows.reshape(tokens, heads, HEAD_DIM))
    return gated.reshape(tokens, heads * HEAD_DIM).astype(jnp.bfloat16)


def local(
    activations,
    norm_gain,
    query_weight,
    key_weight,
    value_weight,
    gate_weight,
    out_weight,
    mlp_gain,
    up_weight,
    down_weight,
):
    full_rows = lax.all_gather(activations, "tp", axis=1, tiled=True)
    normed = rms_norm(full_rows, norm_gain)
    head_width = query_weight.shape[1]
    pieces = (
        lax.all_gather(query_weight, "fs", axis=0, tiled=True),
        lax.all_gather(key_weight, "fs", axis=0, tiled=True),
        lax.all_gather(value_weight, "fs", axis=0, tiled=True),
        lax.all_gather(gate_weight, "fs", axis=0, tiled=True),
    )
    columns = normed
    query_raw, key_raw, value_raw, gate_rows = tuple(
        (jnp.dot(columns, piece, preferred_element_type=jnp.float32) for piece in pieces)
    )
    first_head = (lax.axis_index("tp") * (head_width // HEAD_DIM)).astype(jnp.float32)
    retained = retain(query_raw, key_raw, value_raw.astype(jnp.bfloat16), gate_rows, first_head)
    out_rows = lax.all_gather(out_weight, "fs", axis=1, tiled=True)
    out_mine = lax.all_to_all(out_rows, "tp", split_axis=1, concat_axis=0, tiled=True)
    branch = jnp.dot(
        lax.all_gather(retained, "tp", axis=1, tiled=True),
        out_mine,
        preferred_element_type=jnp.float32,
    )
    middle = (activations.astype(jnp.float32) + branch).astype(jnp.bfloat16)
    middle_rows = lax.all_gather(middle, "tp", axis=1, tiled=True)
    second = rms_norm(middle_rows, mlp_gain)
    columns = second
    up_rows = jnp.dot(
        columns,
        lax.all_gather(up_weight, "fs", axis=0, tiled=True),
        preferred_element_type=jnp.float32,
    )
    hidden = jnp.square(jax.nn.relu(up_rows)).astype(jnp.bfloat16)
    down_part = jnp.dot(
        hidden,
        lax.all_gather(down_weight, "fs", axis=1, tiled=True),
        preferred_element_type=jnp.float32,
    )
    summed = lax.psum_scatter(
        down_part.astype(jnp.bfloat16), "tp", scatter_dimension=1, tiled=True
    ).astype(jnp.float32)
    return (middle.astype(jnp.float32) + summed).astype(jnp.bfloat16)


def solution(mesh):
    in_specs = (
        P(("rep", "fs"), "tp"),
        P(),
        P("fs", "tp"),
        P("fs", "tp"),
        P("fs", "tp"),
        P("fs", "tp"),
        P("tp", "fs"),
        P(),
        P("fs", "tp"),
        P("tp", "fs"),
    )
    out_specs = P(("rep", "fs"), "tp")
    return jax.shard_map(local, mesh=mesh, in_specs=in_specs, out_specs=out_specs, check_vma=False)
```

profile of v0, /device:TPU:0, one launch (start us, length us, event | category | flops | bytes accessed | tf_op | source)
XLA Modules:
  0.0 495.4 jit_solution(16043336632377507980)
XLA Ops:
  6.5 0.7 all-gather.5.cloned.1.call-update
  7.3 1.1 copy.70
  8.3 18.0 %all_gather.36 = bf16[128,2048]{0,1:T(8,128)(2,1)} all-gather(bf16[128,512]{0,1:T(8,128)(2,1)S(1)} %copy.70), channel_id=1, replica_groups=mesh['rep'=2,'fs'=4,'tp'=4] {'fs'}, dimensions={1}, use_global_device_ids=true | all-gather | bytes 655360 | tf_op jit(solution)/shard_map/all_gather | solution.py:126
  26.3 3.5 all-to-all-start
  29.8 0.0 all-gather.7.cloned.1.call-start
  30.0 17.0 %all_gather.32 = bf16[2048,128]{1,0:T(8,128)(2,1)S(1)} all-gather(bf16[512,128]{1,0:T(8,128)(2,1)S(1)} %copy-done.7), channel_id=1, replica_groups=mesh['rep'=2,'fs'=4,'tp'=4] {'fs'}, dimensions={0}, use_global_device_ids=true | all-gather | bytes 655360 | tf_op jit(solution)/shard_map/all_gather | solution.py:115
  47.0 16.0 %all_gather.33 = bf16[2048,128]{1,0:T(8,128)(2,1)S(1)} all-gather(bf16[512,128]{1,0:T(8,128)(2,1)S(1)} %copy-done.8), channel_id=1, replica_groups=mesh['rep'=2,'fs'=4,'tp'=4] {'fs'}, dimensions={0}, use_global_device_ids=true | all-gather | bytes 655360 | tf_op jit(solution)/shard_map/all_gather | solution.py:116
  63.0 16.3 %all_gather.31 = bf16[2048,128]{1,0:T(8,128)(2,1)S(1)} all-gather(bf16[512,128]{1,0:T(8,128)(2,1)S(1)} %copy-done.9), channel_id=1, replica_groups=mesh['rep'=2,'fs'=4,'tp'=4] {'fs'}, dimensions={0}, use_global_device_ids=true | all-gather | bytes 655360 | tf_op jit(solution)/shard_map/all_gather | solution.py:117
  79.2 0.7 multiply_exponential_fusion
  79.9 0.7 fusion.34
  80.7 15.5 %all_gather.34 = bf16[2048,128]{1,0:T(8,128)(2,1)} all-gather(bf16[512,128]{1,0:T(8,128)(2,1)S(1)} %copy-done.10), channel_id=1, replica_groups=mesh['rep'=2,'fs'=4,'tp'=4] {'fs'}, dimensions={0}, use_global_device_ids=true | all-gather | bytes 655360 | tf_op jit(solution)/shard_map/all_gather | solution.py:118
  96.1 0.7 exponential_select_fusion
  96.9 1.0 copy.71
  97.9 1.9 fusion.14
  99.8 0.4 fusion.16
  100.2 0.6 fusion.40
  100.8 0.1 reshape.272
  100.9 0.6 fusion.41
  101.5 0.1 reshape.273
  101.6 0.8 subtract_convert_fusion
  102.4 0.1 reshape.275
  102.5 0.2 copy.53
  102.7 0.1 reshape.276
  102.8 0.2 copy.54
  102.9 0.2 reshape.277
  103.1 0.2 copy.58
  103.3 1.1 reshape.278
  104.4 0.9 copy.59
  105.3 0.6 convolution_convert_fusion.1
  105.9 0.1 reshape.271
  106.1 0.6 copy-done.4
  106.7 0.1 multiply_bitcast_fusion
  106.9 1.9 multiply_bitcast_fusion.1
  108.7 3.4 while.13
  108.7 0.3 convolution_bitcast_fusion.3
  109.1 0.1 copy.96
  109.2 0.7 constant_dynamic-update-slice_fusion.2
  109.9 0.5 convolution_add_fusion.3
  110.4 0.3 convolution_bitcast_fusion.3
  110.8 0.1 copy.96
  110.9 0.7 constant_dynamic-update-slice_fusion.2
  111.6 0.5 convolution_add_fusion.3
  112.1 1.8 fusion.39
  114.0 0.2 copy.65
  114.2 0.1 multiply_reduce_fusion
  114.3 0.9 reshape.274
  115.2 0.1 rsqrt.29
  115.3 0.1 copy.69
  115.5 0.1 div.56
  115.6 0.8 copy.67
  116.4 1.6 multiply_convert_fusion.1
  118.0 6.8 %all_gather.35 = bf16[384,512]{1,0:T(8,128)(2,1)S(1)} all-gather(bf16[384,128]{1,0:T(8,128)(2,1)S(1)} %multiply_convert_fusion.1), channel_id=1, replica_groups=mesh['rep'=2,'fs'=4,'tp'=4] {'tp'}, dimensions={1}, use_global_device_ids=true | all-gather | bytes 491520 | tf_op jit(solution)/shard_map/all_gather | solution.py:129
  124.9 1.1 fusion.23
  126.0 0.0 all-gather.11.cloned.1.call-start
  126.1 0.7 all-gather.11.cloned.1.call-update
  126.8 0.5 all-gather.9.cloned.1.call-update
  127.3 0.2 reduce-scatter.2.cloned.1.call-start
  127.6 18.5 %all-gather.7.cloned.1.call-done = bf16[384,2048]{1,0:T(8,128)(2,1)} async-done(((bf16[384,512]{1,0:T(8,128)(2,1)}), bf16[384,2048]{1,0:T(8,128)(2,1)}) %all-gather.7.cloned.1.call-update) | async-done | bytes 1572880 | tf_op jit(solution)/shard_map/all_gather | solution.py:134
  146.0 1.8 fusion.17
  147.9 149.4 %all-gather.11.cloned.1.call-done = bf16[2048,2048]{1,0:T(8,128)(2,1)} async-done(((bf16[2048,512]{1,0:T(8,128)(2,1)}), bf16[2048,2048]{1,0:T(8,128)(2,1)}) %all-gather.11.cloned.1.call-update) | async-done | bytes 8388624 | tf_op jit(solution)/shard_map/all_gather | solution.py:145
  297.3 149.3 %all-gather.9.cloned.1.call-done = bf16[2048,2048]{1,0:T(8,128)(2,1)} async-done(((bf16[512,2048]{1,0:T(8,128)(2,1)}), bf16[2048,2048]{1,0:T(8,128)(2,1)}) %all-gather.9.cloned.1.call-update) | async-done | bytes 8388624 | tf_op jit(solution)/shard_map/all_gather | solution.py:139
  446.5 14.1 %convolution_convert_fusion = bf16[384,2048]{1,0:T(8,128)(2,1)} fusion(bf16[2048,2048]{1,0:T(8,128)(2,1)} %all-gather.11.cloned.1.call-done, bf16[2048,2048]{1,0:T(8,128)(2,1)} %all-gather.9.cloned.1.call-done, bf16[384,2048]{1,0:T(8,128)(2,1)} %all-gather.7.cloned.1.call-done, f32[2048]{0:T(1024)S(1)} %copy-done.15, f32[384]{0:T(512)S(1)} %add_rsqrt_fusion.1), kind=kOutput, calls=%fused_computation.28 | convolution fusion | flops 6448742400 | bytes 19932672 | tf_op jit(solution)/shard_map/dot_general | solution.py:143
  460.6 26.4 %reduce-scatter.2.cloned.1.call-done = bf16[384,512]{1,0:T(8,128)(2,1)} async-done(((bf16[384,2048]{1,0:T(8,128)(2,1)}), bf16[384,512]{1,0:T(8,128)(2,1)}) %reduce-scatter.2.cloned.1.call-update) | async-done | bytes 393232 | tf_op jit(solution)/shard_map/reduce_scatter | solution.py:148
  487.0 1.8 add_convert_fusion
  (55 shorter events, 0.4 us)
Async XLA Ops:
  6.5 23.5 %copy-start.7 = (bf16[512,128]{1,0:T(8,128)(2,1)S(1)}, bf16[512,128]{1,0:T(8,128)(2,1)}, u32[]{:S(2)}) copy-start(bf16[512,128]{1,0:T(8,128)(2,1)} %param.14) | copy-start | bytes 393220
  6.5 40.5 %copy-start.8 = (bf16[512,128]{1,0:T(8,128)(2,1)S(1)}, bf16[512,128]{1,0:T(8,128)(2,1)}, u32[]{:S(2)}) copy-start(bf16[512,128]{1,0:T(8,128)(2,1)} %param.15) | copy-start | bytes 393220
  6.5 56.4 %copy-start.9 = (bf16[512,128]{1,0:T(8,128)(2,1)S(1)}, bf16[512,128]{1,0:T(8,128)(2,1)}, u32[]{:S(2)}) copy-start(bf16[512,128]{1,0:T(8,128)(2,1)} %param.16) | copy-start | bytes 393220
  6.5 91.3 %all-gather.5.cloned.1.call-start = ((), (), s32[]{:S(2)}) async-start(), calls=%async_computation.2 | async-start | bytes 1966080 | tf_op jit(solution)/shard_map/all_gather | solution.py:111
  7.3 73.4 %copy-start.10 = (bf16[512,128]{1,0:T(8,128)(2,1)S(1)}, bf16[512,128]{1,0:T(8,128)(2,1)}, u32[]{:S(2)}) copy-start(bf16[512,128]{1,0:T(8,128)(2,1)} %param.17) | copy-start | bytes 393220
  26.3 70.5 %all-to-all-start = ((bf16[128,4,512]{0,2,1:T(8,128)(2,1)}), bf16[128,4,512]{0,2,1:T(8,128)(2,1)S(1)}, u32[]{:S(2)}, u32[]{:S(2)}) async-start(bf16[128,4,512]{0,2,1:T(8,128)(2,1)} %bitcast.7), calls=%async_computation | async-start | bytes 1048576 | tf_op jit(solution)/shard_map/all_to_all | solution.py:127
  29.8 116.2 %all-gather.7.cloned.1.call-start = ((), (), s32[]{:S(2)}) async-start(), calls=%async_computation.3 | async-start | bytes 1966080 | tf_op jit(solution)/shard_map/all_gather | solution.py:134
  62.9 36.8 %copy-start.12 = (f32[2048]{0:T(1024)S(1)}, f32[2048]{0:T(1024)}, u32[]{:S(2)}) copy-start(f32[2048]{0:T(1024)} %param.13) | copy-start | bytes 24580
  97.9 1.9 copy-start
  100.8 0.8 copy-start.11
  102.9 3.8 copy-start.3
  103.3 3.4 copy-start.14
  104.4 2.5 copy-start.13
  106.0 0.7 copy-start.4
  112.1 4.3 copy-start.6
  115.5 9.4 %copy-start.2 = (bf16[4,128,512]{2,1,0:T(8,128)(2,1)S(1)}, bf16[4,128,512]{2,1,0:T(8,128)(2,1)}, u32[]{:S(2)}) copy-start(bf16[4,128,512]{2,1,0:T(8,128)(2,1)} %copy.71) | copy-start | bytes 1572868
  115.5 9.4 %copy-start.5 = (bf16[384,512]{1,0:T(8,128)(2,1)S(1)}, bf16[384,512]{1,0:T(8,128)(2,1)}, u32[]{:S(2)}) copy-start(bf16[384,512]{1,0:T(8,128)(2,1)} %param.12) | copy-start | bytes 1179652
  126.0 171.2 %all-gather.11.cloned.1.call-start = ((), (), s32[]{:S(2)}) async-start(), calls=%async_computation.5 | async-start | bytes 10485760 | tf_op jit(solution)/shard_map/all_gather | solution.py:145
  126.8 319.8 %copy-start.15 = (f32[2048]{0:T(1024)S(1)}, f32[2048]{0:T(1024)}, u32[]{:S(2)}) copy-start(f32[2048]{0:T(1024)} %param.19) | copy-start | bytes 24580
  126.8 319.8 %all-gather.9.cloned.1.call-start = ((), (), s32[]{:S(2)}) async-start(), calls=%async_computation.4 | async-start | bytes 10485760 | tf_op jit(solution)/shard_map/all_gather | solution.py:139
  127.3 359.7 %reduce-scatter.2.cloned.1.call-start = ((), (), s32[]{:S(2)}) async-start(), calls=%async_computation.6 | async-start | bytes 1966080 | tf_op jit(solution)/shard_map/reduce_scatter | solution.py:148
  147.8 339.2 %copy-start.1 = (bf16[384,512]{1,0:T(8,128)(2,1)S(1)}, bf16[384,512]{1,0:T(8,128)(2,1)}, u32[]{:S(2)}) copy-start(bf16[384,512]{1,0:T(8,128)(2,1)} %fusion.23) | copy-start | bytes 1179652
Sparse Core Ops, SparseCore 0:
  8.9 22.3 all-gather.4
  126.1 19.8 all-gather.6
  147.6 149.5 all-gather.10
  298.7 147.7 all-gather.8
  460.8 26.1 reduce-scatter.1
where the time goes:
time: 496 us; the launch traced here: 495 us
  waiting for transfers between devices  345 us (70%)
  blocking collectives  89.6 us (18%)
  matrix products  22 us (4%)
  between operations  13.5 us (3%)
  other arithmetic  11.1 us (2%)
  local copies, waits for them, and re-layouts  9.82 us (2%)
    all_gather x1, waiting for transfers between devices, local(): lax.all_gather(down_weight, 'fs', axis=1, tiled=True)  149 us
    all_gather x1, waiting for transfers between devices, local(): lax.all_gather(up_weight, 'fs', axis=0, tiled=True)  149 us
    reduce_scatter x1, waiting for transfers between devices, local(): lax.psum_scatter(down_part.astype(jnp.bfloat16), 'tp', scatter_dimension=...  26.4 us
    all_gather x1, waiting for transfers between devices, local(): middle_rows = lax.all_gather(middle, 'tp', axis=1, tiled=True)  18.5 us
    all_gather x1, blocking collectives, local(): out_rows = lax.all_gather(out_weight, 'fs', axis=1, tiled=True)  18 us
    all_gather x1, blocking collectives, local(): lax.all_gather(query_weight, 'fs', axis=0, tiled=True)  17 us
    all_gather x1, blocking collectives, local(): lax.all_gather(value_weight, 'fs', axis=0, tiled=True)  16.3 us
    all_gather x1, blocking collectives, local(): lax.all_gather(key_weight, 'fs', axis=0, tiled=True)  16 us
  transfers between devices with their start and end apart: 6, of which 4 were waited for; matrix products, arithmetic and copies ran while one was open for 1% of the time, Pallas kernels for 0%

commit v1 on v0

--- a/solution.py
+++ b/solution.py
@@ -8,6 +8,22 @@
 BLOCK = 64
 SEQ_LEN = 128
 EPSILON = 1e-06
+
+
+def collect(x, axis, dim):
+    ways, here, step = (lax.axis_size(axis), lax.axis_index(axis), x.shape[dim])
+    lengths = [n * ways if d == dim else n for d, n in enumerate(x.shape)]
+    full = lax.dynamic_update_slice_in_dim(jnp.zeros(lengths, x.dtype), x, here * step, axis=dim)
+    going_up = going_down = x
+    for far in range(1, ways // 2 + 1):
+        going_up = lax.ppermute(going_up, axis, [(d, (d + 1) % ways) for d in range(ways)])
+        full = lax.dynamic_update_slice_in_dim(full, going_up, (here - far) % ways * step, axis=dim)
+        if 2 * far < ways:
+            going_down = lax.ppermute(going_down, axis, [(d, (d - 1) % ways) for d in range(ways)])
+            full = lax.dynamic_update_slice_in_dim(
+                full, going_down, (here + far) % ways * step, axis=dim
+            )
+    return full
 
 
 def rms_norm(rows, gain):
@@ -134,11 +150,7 @@
     middle_rows = lax.all_gather(middle, "tp", axis=1, tiled=True)
     second = rms_norm(middle_rows, mlp_gain)
     columns = second
-    up_rows = jnp.dot(
-        columns,
-        lax.all_gather(up_weight, "fs", axis=0, tiled=True),
-        preferred_element_type=jnp.float32,
-    )
+    up_rows = jnp.dot(columns, collect(up_weight, "fs", 0), preferred_element_type=jnp.float32)
     hidden = jnp.square(jax.nn.relu(up_rows)).astype(jnp.bfloat16)
     down_part = jnp.dot(
         hidden,

time: 496 us -> 453 us (0.913)
  waiting for transfers between devices: 345 us -> 256 us
  starting transfers between devices: 3.81 us -> 33 us
  local copies, waits for them, and re-layouts: 9.82 us -> 23.7 us
    ppermute x0 -> x3, waiting for transfers between devices: none -> 204 us  [the longest x1 109 us: collect(): lax.ppermute(going_down, axis, [(d, (d - 1) % ways) for d in range(ways)])]
    all_gather x1 -> x0, waiting for transfers between devices: 149 us -> none  [local(): lax.all_gather(up_weight, 'fs', axis=0, tiled=True)]
    all_gather x1, waiting for transfers between devices: 149 us -> 24.5 us  [local(): lax.all_gather(down_weight, 'fs', axis=1, tiled=True)]
    ppermute x0 -> x3, starting transfers between devices: none -> 29.3 us  [the longest x2 26.5 us: collect(): lax.ppermute(going_up, axis, [(d, (d + 1) % ways) for d in range(ways)])]
    all_gather x1, waiting for transfers between devices: 18.5 us -> 0.01 us  [local(): middle_rows = lax.all_gather(middle, 'tp', axis=1, tiled=True)]
    dynamic_update_slice x0 -> x4, local copies, waits for them, and re-layouts: none -> 11 us  [the longest x2 6.31 us: collect(): lax.dynamic_update_slice_in_dim(full, going_up, (here - far) % ways * ste...]
  transfers between devices with their start and end apart: 6 -> 8, of which waited for: 4 -> 5; matrix products, arithmetic and copies ran while one was open for 1% -> 5% of each run, Pallas kernels for 0% -> 0%
where the time goes in v1:
time: 453 us; the launch traced here: 452 us
  waiting for transfers between devices  256 us (57%)
  blocking collectives  89.8 us (20%)
  starting transfers between devices  33 us (7%)
  local copies, waits for them, and re-layouts  23.7 us (5%)
  matrix products  23 us (5%)
  between operations  13.5 us (3%)
  other arithmetic  12.4 us (3%)
    ppermute x1, waiting for transfers between devices, collect(): lax.ppermute(going_down, axis, [(d, (d - 1) % ways) for d in range(ways)])  109 us
    ppermute x2, waiting for transfers between devices, collect(): lax.ppermute(going_up, axis, [(d, (d + 1) % ways) for d in range(ways)])  94.8 us
    reduce_scatter x1, waiting for transfers between devices, local(): lax.psum_scatter(down_part.astype(jnp.bfloat16), 'tp', scatter_dimension=...  26.8 us
    ppermute x2, starting transfers between devices, collect(): lax.ppermute(going_up, axis, [(d, (d + 1) % ways) for d in range(ways)])  26.5 us
    all_gather x1, waiting for transfers between devices, local(): lax.all_gather(down_weight, 'fs', axis=1, tiled=True)  24.5 us
    all_gather x1, blocking collectives, local(): out_rows = lax.all_gather(out_weight, 'fs', axis=1, tiled=True)  18 us
    all_gather x1, blocking collectives, local(): lax.all_gather(query_weight, 'fs', axis=0, tiled=True)  17.2 us
    all_gather x1, blocking collectives, local(): lax.all_gather(key_weight, 'fs', axis=0, tiled=True)  15.8 us
  transfers between devices with their start and end apart: 8, of which 5 were waited for; matrix products, arithmetic and copies ran while one was open for 5% of the time, Pallas kernels for 0%

profile of v1, /device:TPU:0, one launch (start us, length us, event | category | flops | bytes accessed | tf_op | source)
XLA Modules:
  0.0 452.0 jit_solution(17411833199812975011)
XLA Ops:
  6.5 0.7 all-gather.4.cloned.1.call-update
  7.3 1.0 copy.70
  8.3 18.0 %all_gather.33 = bf16[128,2048]{0,1:T(8,128)(2,1)} all-gather(bf16[128,512]{0,1:T(8,128)(2,1)S(1)} %copy.70), channel_id=1, replica_groups=mesh['rep'=2,'fs'=4,'tp'=4] {'fs'}, dimensions={1}, use_global_device_ids=true | all-gather | bytes 655360 | tf_op jit(solution)/shard_map/all_gather | solution.py:142
  26.3 3.6 all-to-all-start
  30.1 17.2 %all_gather.29 = bf16[2048,128]{1,0:T(8,128)(2,1)S(1)} all-gather(bf16[512,128]{1,0:T(8,128)(2,1)} %param.14), channel_id=1, replica_groups=mesh['rep'=2,'fs'=4,'tp'=4] {'fs'}, dimensions={0}, use_global_device_ids=true | all-gather | bytes 655360 | tf_op jit(solution)/shard_map/all_gather | solution.py:131
  47.3 15.8 %all_gather.30 = bf16[2048,128]{1,0:T(8,128)(2,1)S(1)} all-gather(bf16[512,128]{1,0:T(8,128)(2,1)S(1)} %copy-done.5), channel_id=1, replica_groups=mesh['rep'=2,'fs'=4,'tp'=4] {'fs'}, dimensions={0}, use_global_device_ids=true | all-gather | bytes 655360 | tf_op jit(solution)/shard_map/all_gather | solution.py:132
  63.1 15.8 %all_gather.28 = bf16[2048,128]{1,0:T(8,128)(2,1)S(1)} all-gather(bf16[512,128]{1,0:T(8,128)(2,1)S(1)} %copy-done.6), channel_id=1, replica_groups=mesh['rep'=2,'fs'=4,'tp'=4] {'fs'}, dimensions={0}, use_global_device_ids=true | all-gather | bytes 655360 | tf_op jit(solution)/shard_map/all_gather | solution.py:133
  78.9 0.7 multiply_exponential_fusion
  79.6 0.8 fusion.34
  80.4 15.4 %all_gather.31 = bf16[2048,128]{1,0:T(8,128)(2,1)} all-gather(bf16[512,128]{1,0:T(8,128)(2,1)S(1)} %copy-done.7), channel_id=1, replica_groups=mesh['rep'=2,'fs'=4,'tp'=4] {'fs'}, dimensions={0}, use_global_device_ids=true | all-gather | bytes 655360 | tf_op jit(solution)/shard_map/all_gather | solution.py:134
  95.8 0.7 exponential_select_fusion
  96.5 1.0 copy.71
  97.5 1.8 fusion.14
  99.3 1.8 fusion.16
  101.2 0.6 fusion.40
  101.9 0.6 fusion.41
  102.5 0.8 subtract_convert_fusion
  103.3 0.1 reshape.275
  103.4 0.2 copy.53
  103.6 0.1 reshape.276
  103.7 0.2 copy.54
  103.9 0.2 reshape.277
  104.1 0.2 copy.58
  104.3 1.1 reshape.278
  105.3 1.0 copy.59
  106.3 0.6 convolution_convert_fusion.1
  106.9 0.1 reshape.271
  107.0 0.6 copy-done.4
  107.7 0.1 multiply_bitcast_fusion
  107.8 1.9 multiply_bitcast_fusion.1
  109.7 3.4 while.13
  109.7 0.3 convolution_bitcast_fusion.3
  110.0 0.1 copy.96
  110.2 0.7 constant_dynamic-update-slice_fusion.6
  110.9 0.5 convolution_add_fusion.3
  111.4 0.3 convolution_bitcast_fusion.3
  111.7 0.1 copy.96
  111.9 0.7 constant_dynamic-update-slice_fusion.6
  112.6 0.5 convolution_add_fusion.3
  113.1 1.8 fusion.39
  114.9 0.2 copy.65
  115.3 0.1 copy.69
  115.5 0.2 reshape.274
  115.8 0.1 copy.67
  116.0 1.6 multiply_convert_fusion.1
  117.6 7.5 %all_gather.32 = bf16[384,512]{1,0:T(8,128)(2,1)S(1)} all-gather(bf16[384,128]{1,0:T(8,128)(2,1)S(1)} %multiply_convert_fusion.1), channel_id=1, replica_groups=mesh['rep'=2,'fs'=4,'tp'=4] {'tp'}, dimensions={1}, use_global_device_ids=true | all-gather | bytes 491520 | tf_op jit(solution)/shard_map/all_gather | solution.py:145
  125.1 2.1 fusion.23
  127.3 0.7 all-gather.8.cloned.1.call-update
  128.0 1.1 collective-permute-start
  129.1 2.8 collective-permute-start.1
  131.9 62.1 %collective-permute-done = bf16[512,2048]{1,0:T(8,128)(2,1)} collective-permute-done((bf16[512,2048]{1,0:T(8,128)(2,1)S(1)}, bf16[512,2048]{1,0:T(8,128)(2,1)}, u32[]{:S(2)}, u32[]{:S(2)}) %collective-permute-start) | collective-permute-done | bytes 2097184 | tf_op jit(solution)/shard_map/ppermute | solution.py:19
  194.0 25.4 %collective-permute-start.2 = (bf16[512,2048]{1,0:T(8,128)(2,1)}, bf16[512,2048]{1,0:T(8,128)(2,1)}, u32[]{:S(2)}, u32[]{:S(2)}) collective-permute-start(bf16[512,2048]{1,0:T(8,128)(2,1)} %collective-permute-done), channel_id=1, source_target_pairs={{0,4},{4,8},{8,12},{12,0},{1,5},{5,9},{9,13},{13,1},{2,6},{6,10},{... | collective-permute-start | bytes 6291464 | tf_op jit(solution)/shard_map/ppermute | solution.py:19
  219.5 4.3 broadcast_in_dim.25
  223.7 1.5 constant_dynamic-update-slice_fusion.4
  225.3 3.1 constant_dynamic-update-slice_fusion.3
  228.4 108.9 %collective-permute-done.1 = bf16[512,2048]{1,0:T(8,128)(2,1)} collective-permute-done((bf16[512,2048]{1,0:T(8,128)(2,1)S(1)}, bf16[512,2048]{1,0:T(8,128)(2,1)}, u32[]{:S(2)}, u32[]{:S(2)}) %collective-permute-start.1) | collective-permute-done | bytes 2097184 | tf_op jit(solution)/shard_map/ppermute | solution.py:22
  337.3 3.2 constant_dynamic-update-slice_fusion.2
  340.5 32.7 %collective-permute-done.2 = bf16[512,2048]{1,0:T(8,128)(2,1)} collective-permute-done((bf16[512,2048]{1,0:T(8,128)(2,1)}, bf16[512,2048]{1,0:T(8,128)(2,1)}, u32[]{:S(2)}, u32[]{:S(2)}) %collective-permute-start.2) | collective-permute-done | bytes 2097184 | tf_op jit(solution)/shard_map/ppermute | solution.py:19
  373.2 3.2 constant_dynamic-update-slice_fusion.1
  376.3 1.8 fusion.17
  378.1 24.5 %all-gather.8.cloned.1.call-done = bf16[2048,2048]{1,0:T(8,128)(2,1)} async-done(((bf16[2048,512]{1,0:T(8,128)(2,1)}), bf16[2048,2048]{1,0:T(8,128)(2,1)}) %all-gather.8.cloned.1.call-update) | async-done | bytes 8388624 | tf_op jit(solution)/shard_map/all_gather | solution.py:157
  402.6 14.1 %convolution_convert_fusion = bf16[384,2048]{1,0:T(8,128)(2,1)} fusion(bf16[2048,2048]{1,0:T(8,128)(2,1)} %all-gather.8.cloned.1.call-done, bf16[2048,2048]{1,0:T(8,128)(2,1)} %constant_dynamic-update-slice_fusion.1, bf16[384,2048]{1,0:T(8,128)(2,1)} %all-gather.6.cloned.1.call-done, f32[2048]{0:T(1024)S(1)} %copy-done.12, f32[384]{0:T(512)S(1)} %add_rsqrt_fusion.1), kind=kOutput, calls=%fused_computation.28 | convolution fusion | flops 6448742400 | bytes 19932672 | tf_op jit(solution)/shard_map/dot_general | solution.py:155
  416.8 26.8 %reduce-scatter.2.cloned.1.call-done = bf16[384,512]{1,0:T(8,128)(2,1)} async-done(((bf16[384,2048]{1,0:T(8,128)(2,1)}), bf16[384,512]{1,0:T(8,128)(2,1)}) %reduce-scatter.2.cloned.1.call-update) | async-done | bytes 393232 | tf_op jit(solution)/shard_map/reduce_scatter | solution.py:160
  443.6 1.8 add_convert_fusion
  (57 shorter events, 0.8 us)
Async XLA Ops:
  6.5 40.7 %copy-start.5 = (bf16[512,128]{1,0:T(8,128)(2,1)S(1)}, bf16[512,128]{1,0:T(8,128)(2,1)}, u32[]{:S(2)}) copy-start(bf16[512,128]{1,0:T(8,128)(2,1)} %param.15) | copy-start | bytes 393220
  6.5 56.6 %copy-start.6 = (bf16[512,128]{1,0:T(8,128)(2,1)S(1)}, bf16[512,128]{1,0:T(8,128)(2,1)}, u32[]{:S(2)}) copy-start(bf16[512,128]{1,0:T(8,128)(2,1)} %param.16) | copy-start | bytes 393220
  6.5 73.8 %copy-start.7 = (bf16[512,128]{1,0:T(8,128)(2,1)S(1)}, bf16[512,128]{1,0:T(8,128)(2,1)}, u32[]{:S(2)}) copy-start(bf16[512,128]{1,0:T(8,128)(2,1)} %param.17) | copy-start | bytes 393220
  6.5 91.0 %all-gather.4.cloned.1.call-start = ((), (), s32[]{:S(2)}) async-start(), calls=%async_computation.2 | async-start | bytes 1966080 | tf_op jit(solution)/shard_map/all_gather | solution.py:127
  26.3 73.0 %copy-start.9 = (f32[2048]{0:T(1024)S(1)}, f32[2048]{0:T(1024)}, u32[]{:S(2)}) copy-start(f32[2048]{0:T(1024)} %param.13) | copy-start | bytes 24580
  26.3 70.2 %all-to-all-start = ((bf16[128,4,512]{0,2,1:T(8,128)(2,1)}), bf16[128,4,512]{0,2,1:T(8,128)(2,1)S(1)}, u32[]{:S(2)}, u32[]{:S(2)}) async-start(bf16[128,4,512]{0,2,1:T(8,128)(2,1)} %bitcast.7), calls=%async_computation | async-start | bytes 1048576 | tf_op jit(solution)/shard_map/all_to_all | solution.py:143
  29.9 346.4 %all-gather.6.cloned.1.call-start = ((), (), s32[]{:S(2)}) async-start(), calls=%async_computation.3 | async-start | bytes 1966080 | tf_op jit(solution)/shard_map/all_gather | solution.py:150
  101.8 0.8 copy-start.8
  103.3 4.3 copy-start.11
  103.6 4.2 copy-start.10
  103.9 3.9 copy-start.3
  107.0 0.7 copy-start.4
  114.9 10.2 %copy-start.2 = (bf16[4,128,512]{2,1,0:T(8,128)(2,1)S(1)}, bf16[4,128,512]{2,1,0:T(8,128)(2,1)}, u32[]{:S(2)}) copy-start(bf16[4,128,512]{2,1,0:T(8,128)(2,1)} %copy.71) | copy-start | bytes 1572868
  117.6 10.4 %copy-start.1 = (bf16[512,2048]{1,0:T(8,128)(2,1)S(1)}, bf16[512,2048]{1,0:T(8,128)(2,1)}, u32[]{:S(2)}) copy-start(bf16[512,2048]{1,0:T(8,128)(2,1)} %param.20) | copy-start | bytes 6291460
  127.2 275.4 %all-gather.8.cloned.1.call-start = ((), (), s32[]{:S(2)}) async-start(), calls=%async_computation.4 | async-start | bytes 10485760 | tf_op jit(solution)/shard_map/all_gather | solution.py:157
  128.0 315.6 %reduce-scatter.2.cloned.1.call-start = ((), (), s32[]{:S(2)}) async-start(), calls=%async_computation.5 | async-start | bytes 1966080 | tf_op jit(solution)/shard_map/reduce_scatter | solution.py:160
  128.0 66.0 %collective-permute-start = (bf16[512,2048]{1,0:T(8,128)(2,1)S(1)}, bf16[512,2048]{1,0:T(8,128)(2,1)}, u32[]{:S(2)}, u32[]{:S(2)}) collective-permute-start(bf16[512,2048]{1,0:T(8,128)(2,1)S(1)} %copy-done.1), channel_id=1, source_target_pairs={{0,4},{4,8},{8,12},{12,0},{1,5},{5,9},{9,13},{13,1},{2,6},{6,10},{... | collective-permute-start | bytes 6291464 | tf_op jit(solution)/shard_map/ppermute | solution.py:19
  129.1 208.2 %collective-permute-start.1 = (bf16[512,2048]{1,0:T(8,128)(2,1)S(1)}, bf16[512,2048]{1,0:T(8,128)(2,1)}, u32[]{:S(2)}, u32[]{:S(2)}) collective-permute-start(bf16[512,2048]{1,0:T(8,128)(2,1)S(1)} %copy-done.1), channel_id=1, source_target_pairs={{0,12},{4,0},{8,4},{12,8},{1,13},{5,1},{9,5},{13,9},{2,14},{6,2},{... | collective-permute-start | bytes 6291464 | tf_op jit(solution)/shard_map/ppermute | solution.py:22
  194.0 179.1 %collective-permute-start.2 = (bf16[512,2048]{1,0:T(8,128)(2,1)}, bf16[512,2048]{1,0:T(8,128)(2,1)}, u32[]{:S(2)}, u32[]{:S(2)}) collective-permute-start(bf16[512,2048]{1,0:T(8,128)(2,1)} %collective-permute-done), channel_id=1, source_target_pairs={{0,4},{4,8},{8,12},{12,0},{1,5},{5,9},{9,13},{13,1},{2,6},{6,10},{... | collective-permute-start | bytes 6291464 | tf_op jit(solution)/shard_map/ppermute | solution.py:19
  340.5 62.2 %copy-start.12 = (f32[2048]{0:T(1024)S(1)}, f32[2048]{0:T(1024)}, u32[]{:S(2)}) copy-start(f32[2048]{0:T(1024)} %param.19) | copy-start | bytes 24580
  378.1 65.5 %copy-start = (bf16[384,512]{1,0:T(8,128)(2,1)S(1)}, bf16[384,512]{1,0:T(8,128)(2,1)}, u32[]{:S(2)}) copy-start(bf16[384,512]{1,0:T(8,128)(2,1)} %fusion.23) | copy-start | bytes 1179652
Sparse Core Ops, SparseCore 0:
  8.9 22.3 all-gather.3
  127.3 19.9 all-gather.5
  148.9 253.7 all-gather.7
  416.9 26.6 reduce-scatter.1
